TPU v7x, 32 devices: a whole 2x2x4 slice. The times are simulated.
32 devices in a mesh: fs: 16 (over z, y, x), tp: 2 (over core).
Axes of the slice: x: 2, y: 2, z: 4, core: 2. Of those that a mesh axis runs over, the one named last changes fastest.
Arguments:
- tokens: bfloat16 [2048, 2048], P('fs', 'tp'), may hold values from -300 to 300
- norm_gain: float32 [2048], P('fs'), may hold values from 0.1 to 1.9
- gate_weight: float32 [16, 2048, 1024], P(None, 'fs', 'tp'), may hold values from -1.3258252 to 1.3258252
- up_weight: float32 [16, 2048, 1024], P(None, 'fs', 'tp'), may hold values from -1.3258252 to 1.3258252
- down_weight: float32 [16, 1024, 2048], P(None, 'fs', 'tp'), may hold values from -0.1875 to 0.1875
- routes: int32 [2048, 4], P('fs'), may hold values from 0 to 15, all different within a row; in each aligned block of 128 rows (0 to 127, 128 to 255, ...) at most 64 rows name the same one
- route_weights: float32 [2048, 4], P('fs'), may hold values from 0.05 to 1
Outputs:
- mixed: bfloat16 [2048, 2048], P('fs', 'tp')
- gate_ready: bfloat16 [16, 2048, 1024], P('fs', None, 'tp')
- up_ready: bfloat16 [16, 2048, 1024], P('fs', None, 'tp')
- down_ready: bfloat16 [16, 1024, 2048], P('fs', None, 'tp')
Inputs may be any that keep to these rules, and one draw needn't show every extreme that they name: `routes`: each row names 4 different experts. In each aligned block of 128 rows no expert is named more than 64 times, a bound that some block reaches.
All inputs are finite; a program needn't handle non-finite values.
Results may differ from a plain program's by a relative error of at most 0.0089.
Values may be sent and summed in bfloat16 or wider, within the bound.
A program may use at most 64 MiB of HBM per device.

v0:
```python
import functools

import jax
import jax.numpy as jnp
from jax import lax
from jax.experimental import pallas as pl
from jax.experimental.pallas import tpu as pltpu
from jax.sharding import PartitionSpec as P

epsilon = 1e-05
MESH = pl.DeviceIdType.MESH
GROUPS = 4


def activate(gate_pre, up_pre):
    gated = jnp.minimum(gate_pre, 7.0)
    upper = jnp.clip(up_pre, -7.0, 7.0)
    return (upper + 1.0) * gated * jax.nn.sigmoid(1.702 * gated)


def kernel(
    n, cores, slots_in, gate_in, up_in, down_in, mix_high, mix_low,
    mixed_out, gate_out, up_out, down_out,
    rows, gate, up, down, hidden, results, back,
    send_sem, recv_sem, own_sem, out_sem, tp_send, tp_recv,
):
    me = lax.axis_index("fs")
    core = lax.axis_index("tp")
    depth = gate_in.shape[1]
    units = down_in.shape[1]
    items = slots_in.shape[1]
    total = n * items
    width = slots_in.shape[2]
    columns = gate_in.shape[2]

    barrier = pltpu.get_barrier_semaphore()

    def greet(step, carry):
        pl.semaphore_signal(barrier, inc=1, device_id={"fs": lax.rem(me + step, n)}, device_id_type=MESH)
        return carry

    lax.fori_loop(1, n, greet, 0)
    for step in range(1, cores):
        pl.semaphore_signal(barrier, inc=1, device_id={"tp": lax.rem(core + step, cores)}, device_id_type=MESH)
    pl.semaphore_wait(barrier, n - 1 + cores - 1)

    mine = rows.at[core]
    phases = ((slots_in, mine, items), (gate_in, gate, depth), (up_in, up, depth), (down_in, down, units))

    def own(phase):
        source, landing, size = phases[phase]
        return pltpu.make_async_copy(source.at[me], landing.at[pl.ds(me * size, size)], own_sem.at[phase])

    def start(phase):
        source, landing, size = phases[phase]

        def send(step, carry):
            peer = lax.rem(me + step, n)
            pltpu.make_async_remote_copy(
                src_ref=source.at[peer],
                dst_ref=landing.at[pl.ds(me * size, size)],
                send_sem=send_sem.at[phase],
                recv_sem=recv_sem.at[phase],
                device_id={"fs": peer},
                device_id_type=MESH,
            ).start()
            return carry

        own(phase).start()
        lax.fori_loop(1, n, send, 0)

    def drain(landing, size, semaphore):
        piece = landing.at[pl.ds(0, (n - 1) * size)]
        pltpu.make_async_copy(piece, piece, semaphore).wait()

    def arrive(phase):
        _, landing, size = phases[phase]
        drain(landing, size, recv_sem.at[phase])
        own(phase).wait()

    def swap(buffer, slot):
        copies = []
        for step in range(1, cores):
            copies.append(
                pltpu.make_async_remote_copy(
                    src_ref=buffer.at[core],
                    dst_ref=buffer.at[core],
                    send_sem=tp_send.at[slot, step - 1],
                    recv_sem=tp_recv.at[slot, step - 1],
                    device_id={"tp": lax.rem(core + step, cores)},
                    device_id_type=MESH,
                )
            )
        for copy in copies:
            copy.start()
        return copies

    for phase in range(4):
        start(phase)

    arrive(0)
    swapped = swap(rows, 0)
    arrive(1)
    gate_copy = pltpu.make_async_copy(gate, gate_out, out_sem.at[0])
    gate_copy.start()
    for copy in swapped:
        copy.wait()
    arrive(2)
    up_copy = pltpu.make_async_copy(up, up_out, out_sem.at[1])
    up_copy.start()

    tile = total // GROUPS

    def first_layer(group, carry):
        at = pl.ds(pl.multiple_of(group * tile, tile), tile)
        gate_pre = jnp.zeros((tile, columns), jnp.float32)
        up_pre = jnp.zeros((tile, columns), jnp.float32)
        for part in range(cores):
            block = rows[part, at, :]
            span = pl.ds(part * width, width)
            gate_pre = gate_pre + jnp.dot(block, gate[span, :], preferred_element_type=jnp.float32)
            up_pre = up_pre + jnp.dot(block, up[span, :], preferred_element_type=jnp.float32)
        hidden[core, at, :] = activate(gate_pre, up_pre).astype(jnp.bfloat16)
        return carry

    lax.fori_loop(0, GROUPS, first_layer, 0)
    swapped = swap(hidden, 1)
    for copy in swapped:
        copy.wait()
    arrive(3)
    down_copy = pltpu.make_async_copy(down, down_out, out_sem.at[2])
    down_copy.start()

    share = n // GROUPS
    home = me // share

    def second_layer(turn, carry):
        group = lax.rem(home + 1 + turn, GROUPS)
        at = pl.ds(pl.multiple_of(group * tile, tile), tile)
        summed = jnp.zeros((tile, width), jnp.float32)
        for part in range(cores):
            summed = summed + jnp.dot(
                hidden[part, at, :], down[pl.ds(part * columns, columns), :], preferred_element_type=jnp.float32
            )
        results[at, :] = summed.astype(jnp.bfloat16)

        def give(step, inner):
            peer = group * share + lax.rem(me + step, share)

            @pl.when(peer != me)
            def _():
                pltpu.make_async_remote_copy(
                    src_ref=results.at[pl.ds(peer * items, items)],
                    dst_ref=back.at[pl.ds(me * items, items)],
                    send_sem=send_sem.at[4],
                    recv_sem=recv_sem.at[4],
                    device_id={"fs": peer},
                    device_id_type=MESH,
                ).start()

            return inner

        lax.fori_loop(0, share, give, 0)
        return carry

    lax.fori_loop(0, GROUPS, second_layer, 0)
    kept = pltpu.make_async_copy(
        results.at[pl.ds(me * items, items)], back.at[pl.ds(me * items, items)], own_sem.at[4]
    )
    kept.start()
    kept.wait()
    gate_copy.wait()
    up_copy.wait()
    down_copy.wait()
    for phase in range(4):
        source, landing, size = phases[phase]
        drain(landing, size, send_sem.at[phase])
    drain(back, items, send_sem.at[4])
    drain(back, items, recv_sem.at[4])
    mixed = jnp.dot(mix_high[...], back[...], preferred_element_type=jnp.float32)
    mixed = mixed + jnp.dot(mix_low[...], back[...], preferred_element_type=jnp.float32)
    mixed_out[...] = mixed.astype(jnp.bfloat16)


def shards(n, cores, tokens, norm_gain, gate_weight, up_weight, down_weight, routes, route_weights):
    experts, depth, columns = gate_weight.shape
    units, width = down_weight.shape[1:]
    tok_rows, top_count = routes.shape
    items = 2 * tok_rows * top_count // experts
    total = experts * items
    gate_send = (norm_gain[None, :, None] * gate_weight).astype(jnp.bfloat16)
    up_send = (norm_gain[None, :, None] * up_weight).astype(jnp.bfloat16)
    down_send = down_weight.astype(jnp.bfloat16)

    values = tokens.astype(jnp.float32)
    squared = lax.psum(jnp.sum(values * values, axis=1), "tp")
    normed = (values * lax.rsqrt(squared / (width * cores) + epsilon)[:, None]).astype(jnp.bfloat16)

    names = jnp.arange(experts, dtype=jnp.int32)
    hits = routes[:, :, None] == names[None, None, :]
    member = jnp.any(hits, axis=1)
    weight = jnp.sum(jnp.where(hits, route_weights[:, :, None], 0.0), axis=1)
    order = jnp.arange(tok_rows, dtype=jnp.int32)
    earlier = (order[:, None] > order[None, :]).astype(jnp.bfloat16)
    place = jnp.dot(earlier, member.astype(jnp.bfloat16), preferred_element_type=jnp.float32).astype(jnp.int32)
    place = jnp.where(member, place, -1)
    slots = jnp.arange(items, dtype=jnp.int32)
    chosen = place.T[:, None, :] == slots[None, :, None]
    picks = chosen.astype(jnp.bfloat16).reshape(total, tok_rows)
    outbound = jnp.dot(picks, normed, preferred_element_type=jnp.float32).astype(jnp.bfloat16)
    rounded = lax.reduce_precision(weight, 8, 7)
    high = rounded.astype(jnp.bfloat16)
    low = (weight - rounded).astype(jnp.bfloat16)
    at_slot = place[:, :, None] == slots[None, None, :]
    zero = jnp.zeros((), jnp.bfloat16)
    mix_high = jnp.where(at_slot, high[:, :, None], zero).reshape(tok_rows, total)
    mix_low = jnp.where(at_slot, low[:, :, None], zero).reshape(tok_rows, total)

    anywhere = pl.BlockSpec(memory_space=pl.ANY)
    near = pl.BlockSpec(memory_space=pltpu.VMEM)
    mixed, gate_ready, up_ready, down_ready = pl.pallas_call(
        functools.partial(kernel, n, cores),
        out_shape=(
            jax.ShapeDtypeStruct((tok_rows, width), jnp.bfloat16),
            jax.ShapeDtypeStruct((n * depth, columns), jnp.bfloat16),
            jax.ShapeDtypeStruct((n * depth, columns), jnp.bfloat16),
            jax.ShapeDtypeStruct((n * units, width), jnp.bfloat16),
        ),
        in_specs=[anywhere] * 4 + [near] * 2,
        out_specs=(near, anywhere, anywhere, anywhere),
        scratch_shapes=[
            pltpu.VMEM((cores, total, width), jnp.bfloat16),
            pltpu.VMEM((n * depth, columns), jnp.bfloat16),
            pltpu.VMEM((n * depth, columns), jnp.bfloat16),
            pltpu.VMEM((n * units, width), jnp.bfloat16),
            pltpu.VMEM((cores, total, columns), jnp.bfloat16),
            pltpu.VMEM((total, width), jnp.bfloat16),
            pltpu.VMEM((total, width), jnp.bfloat16),
            pltpu.SemaphoreType.DMA((5,)),
            pltpu.SemaphoreType.DMA((5,)),
            pltpu.SemaphoreType.DMA((5,)),
            pltpu.SemaphoreType.DMA((3,)),
            pltpu.SemaphoreType.DMA((2, cores - 1)),
            pltpu.SemaphoreType.DMA((2, cores - 1)),
        ],
        compiler_params=pltpu.CompilerParams(
            collective_id=0, has_side_effects=True, vmem_limit_bytes=40 * 1024 * 1024
        ),
    )(outbound.reshape(experts, items, width), gate_send, up_send, down_send, mix_high, mix_low)
    return (mixed, gate_ready[None], up_ready[None], down_ready[None])


def solution(mesh):
    placed = (
        P("fs", "tp"),
        P("fs"),
        P(None, "fs", "tp"),
        P(None, "fs", "tp"),
        P(None, "fs", "tp"),
        P("fs", None),
        P("fs", None),
    )
    return jax.shard_map(
        functools.partial(shards, mesh.shape["fs"], mesh.shape["tp"]),
        mesh=mesh,
        in_specs=placed,
        out_specs=(P("fs", "tp"), P("fs", None, "tp"), P("fs", None, "tp"), P("fs", None, "tp")),
        check_vma=False,
    )
```

profile of v0, /device:TPU:20, one launch (start us, length us, event | category | flops | bytes accessed | tf_op | source)
XLA Modules:
  0.0 269.8 jit_solution(7872871931287906179)
XLA Ops:
  0.6 1.1 fusion.1
  1.7 2.5 psum.7
  4.2 0.7 fusion.5
  4.9 0.1 fusion
  5.0 0.7 select_reduce_fusion
  5.8 0.1 eq.60
  5.8 0.2 bitcast_compare_fusion
  6.1 0.1 copy.20
  6.2 0.0 copy-start.2
  6.3 0.1 copy.21
  6.5 0.2 copy.19
  6.7 0.0 copy-start
  6.7 0.1 broadcast_select_fusion
  6.9 0.3 copy-done.2
  7.2 0.8 convolution_convert_fusion
  8.0 0.9 copy-done
  8.9 1.6 convert_element_type.46.down_in
  10.6 1.3 copy-done.1
  11.9 3.5 %multiply_convert_fusion = (bf16[16,128,512]{2,1,0:T(8,128)(2,1)S(1)}, bf16[16,128,512]{2,1,0:T(8,128)(2,1)S(1)}) fusion(f32[16,128,512]{2,1,0:T(8,128)S(1)} %copy-done.1, f32[128]{0:T(128)S(1)} %copy-done.3, f32[16,128,512]{2,1,0:T(8,128)} %param.9), kind=kLoop, calls=%fused_computation | loop fusion | flops 4194304 | bytes 12583424 | tf_op jit(solution)/shard_map/convert_element_type | solution.py:192
  15.4 249.7 %shard_map.102 = (bf16[128,1024]{1,0:T(8,128)(2,1)S(1)}, bf16[2048,512]{1,0:T(8,128)(2,1)S(1)}, bf16[2048,512]{1,0:T(8,128)(2,1)S(1)}, bf16[1024,1024]{1,0:T(8,128)(2,1)S(1)}) custom-call(bf16[16,64,1024]{2,1,0:T(8,128)(2,1)S(1)} %bitcast.12, bf16[16,128,512]{2,1,0:T(8,128)(2,1)S(1)} %get-tuple-element.17.gate_in, ...), custom_call_target="tpu_custom_call" | custom-call | tf_op jit(solution)/shard_map/pallas_call | solution.py:221
  265.1 0.7 copy.28
  265.8 1.3 copy.29
  267.1 1.3 copy.30
  268.4 1.3 copy.31
  (10 shorter events, 0.2 us)
Async XLA Ops:
  6.2 1.0 copy-start.2
  6.7 2.2 copy-start
  8.9 2.9 %copy-start.1 = (f32[16,128,512]{2,1,0:T(8,128)S(1)}, f32[16,128,512]{2,1,0:T(8,128)}, u32[]{:S(2)}) copy-start(f32[16,128,512]{2,1,0:T(8,128)} %param.10) | copy-start | bytes 12582916
  8.9 2.9 %copy-start.3 = (f32[128]{0:T(128)S(1)}, f32[128]{0:T(128)}, u32[]{:S(2)}) copy-start(f32[128]{0:T(128)} %param.8) | copy-start | bytes 1540
where the time goes:
time: 270 us
  Pallas kernels  250 us (93%)
  other arithmetic  8.04 us (3%)
  local copies, waits for them, and re-layouts  7.89 us (3%)
    pallas_call x1, Pallas kernels, shards(): pl.pallas_call(functools.partial(kernel, n, cores), out_shape=(jax.ShapeD...  250 us
    unnamed x12, local copies, waits for them, and re-layouts  7.22 us

commit v1 on v0

v1 whole, which is shorter than its diff:
```python
import functools
import math

import jax
import jax.numpy as jnp
from jax import lax
from jax.experimental import pallas as pl
from jax.experimental.pallas import tpu as pltpu
from jax.sharding import PartitionSpec as P

epsilon = 1e-05
MESH = pl.DeviceIdType.MESH
CHUNKS = 4
PIECES = 4
WINDOW = 3


def activate(gate_pre, up_pre):
    gated = jnp.minimum(gate_pre, 7.0)
    upper = jnp.clip(up_pre, -7.0, 7.0)
    return (upper + 1.0) * gated * jax.nn.sigmoid(1.702 * gated)


def plane_size(n):
    return max(size for size in range(1, math.isqrt(n) + 1) if n % size == 0 and (n // size) % 2 == 0)


def kernel(
    n, cores, items, pieces, chunks,
    tokens_in, gain_in, gate_in, up_in, down_in, routes_in, weights_in,
    mixed_out, gate_out, up_out, down_out,
    tok_raw, gain_row, gain_tile, routes_v, weights_v, square,
    gate_f, up_f, down_f, gate_s, up_s, down_s, gate, up, down,
    block, info, mix_high, mix_low, picked, rows, hidden,
    results, back, part_f, part_s, lead_in, half_in, cross, cross_in, mixed,
    load_sem, w_send, w_recv, t_send, near_recv, far_recv, fwd_send, p_sem, tp_send, tp_recv,
    r_send, r_recv, h_send, h_recv, l_send, l_recv, x_send, x_recv, out_sem,
):
    me = lax.axis_index("fs")
    core = lax.axis_index("tp")
    plane = plane_size(n)
    depths = n // plane
    half = depths // 2
    z = me // plane
    q = lax.rem(me, plane)
    base = (z // half) * half
    other = half - base
    leader = half - 1 + z // half
    other_leader = half - z // half
    place_in_half = z - base

    tok_rows, width = tokens_in.shape
    depth, columns = gate_in.shape[1:]
    units = down_in.shape[1]
    piece = depth // pieces
    chunk = width // chunks
    top_count = routes_in.shape[0]

    def fs(index):
        return {"fs": index}

    def remote(source, landing, sent, received, where):
        pltpu.make_async_remote_copy(
            src_ref=source, dst_ref=landing, send_sem=sent, recv_sem=received,
            device_id=where, device_id_type=MESH,
        ).start()

    def drain(ref, semaphore):
        pltpu.make_async_copy(ref, ref, semaphore).wait()

    small = ((tokens_in, tok_raw), (gain_in, gain_row), (routes_in, routes_v), (weights_in, weights_v))
    loads = [pltpu.make_async_copy(source, landing, load_sem.at[i]) for i, (source, landing) in enumerate(small)]
    phases = []
    for source, staged, sent, landing in ((gate_in, gate_f, gate_s, gate), (up_in, up_f, up_s, up)):
        for p in range(pieces):
            phases.append((
                source.at[:, pl.ds(p * piece, piece)], staged.at[p], sent.at[p],
                landing, depth, p * piece, piece, True,
            ))
    for c in range(chunks):
        phases.append((
            down_in.at[:, :, pl.ds(c * chunk, chunk)], down_f.at[c], down_s.at[c],
            down.at[c], units, 0, units, False,
        ))
    weight_loads = [
        pltpu.make_async_copy(phase[0], phase[1], load_sem.at[len(small) + i]) for i, phase in enumerate(phases)
    ]
    loads[1].start()
    weight_loads[0].start()
    for at in (0, 2, 3):
        loads[at].start()
    for copy in weight_loads[1:]:
        copy.start()

    barrier = pltpu.get_barrier_semaphore()

    def greet(step, carry):
        pl.semaphore_signal(barrier, inc=1, device_id=fs(lax.rem(me + step, n)), device_id_type=MESH)
        return carry

    lax.fori_loop(1, n, greet, 0)
    for step in range(1, cores):
        pl.semaphore_signal(barrier, inc=1, device_id={"tp": lax.rem(core + step, cores)}, device_id_type=MESH)

    loads[1].wait()
    row_at = lax.broadcasted_iota(jnp.int32, (depth, depth), 0)
    lane_at = lax.broadcasted_iota(jnp.int32, (depth, depth), 1)
    spread = jnp.where(row_at == lane_at, jnp.broadcast_to(gain_row[...], (depth, depth)), 0.0)
    gain_tile[...] = jnp.broadcast_to(jnp.sum(spread, axis=1, keepdims=True), gain_tile.shape)

    def cast(index):
        _, staged, sent, landing, stride, offset, size, scaled = phases[index]
        weight_loads[index].wait()

        def rounded(peer):
            value = staged[peer]
            if scaled:
                lanes = gain_tile.shape[1]
                gain = gain_tile[offset:offset + size, :]
                value = value * jnp.concatenate([gain] * (value.shape[1] // lanes), axis=1)
            return value.astype(jnp.bfloat16)

        def one(step, carry):
            peer = lax.rem(me + step, n)
            sent[peer] = rounded(peer)
            return carry

        lax.fori_loop(1, n, one, 0)
        landing[pl.ds(pl.multiple_of(me * stride + offset, size), size), :] = rounded(me)

    def send(index):
        _, _, sent, landing, stride, offset, size, _ = phases[index]

        def one(step, carry):
            peer = lax.rem(me + step, n)
            remote(
                sent.at[peer], landing.at[pl.ds(pl.multiple_of(me * stride + offset, size), size)],
                w_send.at[index], w_recv.at[index], fs(peer),
            )
            return carry

        lax.fori_loop(1, n, one, 0)

    def arrive(index):
        _, _, _, landing, _, _, size, _ = phases[index]
        drain(landing.at[pl.ds(0, (n - 1) * size)], w_recv.at[index])
        if index + WINDOW < len(phases):
            send(index + WINDOW)

    def swap(buffer, slot):
        copies = []
        for step in range(1, cores):
            copies.append(
                pltpu.make_async_remote_copy(
                    src_ref=buffer.at[core], dst_ref=buffer.at[core],
                    send_sem=tp_send.at[slot, step - 1], recv_sem=tp_recv.at[slot, step - 1],
                    device_id={"tp": lax.rem(core + step, cores)}, device_id_type=MESH,
                )
            )
        for copy in copies:
            copy.start()
        return copies

    cast(0)
    loads[0].wait()
    values = tok_raw[...].astype(jnp.float32)
    square[core] = jnp.broadcast_to(jnp.sum(values * values, axis=1, keepdims=True), square.shape[1:])
    pl.semaphore_wait(barrier, n - 1 + cores - 1)
    send(0)
    swapped = swap(square, 0)

    loads[2].wait()
    loads[3].wait()
    names = lax.broadcasted_iota(jnp.int32, (n, tok_rows), 0)
    weight = jnp.zeros((n, tok_rows), jnp.float32)
    member = jnp.zeros((n, tok_rows), jnp.float32)
    for k in range(top_count):
        hit = jnp.broadcast_to(routes_v[k:k + 1, :], (n, tok_rows)) == names
        weight = weight + jnp.where(hit, jnp.broadcast_to(weights_v[k:k + 1, :], (n, tok_rows)), 0.0)
        member = member + jnp.where(hit, 1.0, 0.0)
    before = lax.broadcasted_iota(jnp.int32, (tok_rows, tok_rows), 0)
    after = lax.broadcasted_iota(jnp.int32, (tok_rows, tok_rows), 1)
    earlier = jnp.where(before < after, 1.0, 0.0).astype(jnp.bfloat16)
    place = jnp.dot(member.astype(jnp.bfloat16), earlier, preferred_element_type=jnp.float32)
    place = jnp.where(member > 0.0, place, -1.0)
    for p in range(depths):
        info[z, 0, p] = weight[p * plane:(p + 1) * plane]
        info[z, 1, p] = place[p * plane:(p + 1) * plane]

    for copy in swapped:
        copy.wait()
    total = square[0]
    for part in range(1, cores):
        total = total + square[part]
    scale = lax.rsqrt(total / (width * cores) + epsilon)
    values = tok_raw[...].astype(jnp.float32)
    lanes = scale.shape[1]
    block[z] = (values * jnp.concatenate([scale] * (width // lanes), axis=1)).astype(jnp.bfloat16)

    def give_tokens(dest, received):
        remote(block.at[z], block.at[z], t_send.at[0], received.at[0], fs(dest * plane + q))
        remote(info.at[z], info.at[z], t_send.at[1], received.at[1], fs(dest * plane + q))

    give_tokens(other_leader, far_recv)
    for step in range(1, half):
        give_tokens(base + lax.rem(place_in_half + step, half), near_recv)
    for index in range(1, min(WINDOW, len(phases))):
        cast(index)
        send(index)
    for index in range(WINDOW, len(phases)):
        cast(index)

    def take_far():
        drain(block.at[pl.ds(0, half)], far_recv.at[0])
        drain(info.at[pl.ds(0, half)], far_recv.at[1])

    def forward():
        @pl.when(z == leader)
        def _():
            take_far()
            for step in range(1, half):
                dest = fs((base + lax.rem(place_in_half + step, half)) * plane + q)
                remote(block.at[pl.ds(other, half)], block.at[pl.ds(other, half)], fwd_send.at[0], far_recv.at[0], dest)
                remote(info.at[pl.ds(other, half)], info.at[pl.ds(other, half)], fwd_send.at[1], far_recv.at[1], dest)

    own_pick = pltpu.make_async_copy(picked.at[q], rows.at[core, q], p_sem.at[2])

    def dispatch():
        @pl.when(z != leader)
        def _():
            take_far()

        if half > 1:
            drain(block.at[pl.ds(0, half - 1)], near_recv.at[0])
            drain(info.at[pl.ds(0, half - 1)], near_recv.at[1])
        slot = lax.broadcasted_iota(jnp.int32, (items, tok_rows), 0).astype(jnp.float32)

        def one(source, carry):
            weights = info[source, 0, z]
            places = info[source, 1, z]
            chosen, mixing = [], []
            for j in range(plane):
                at = jnp.broadcast_to(places[j:j + 1, :], (items, tok_rows)) == slot
                chosen.append(jnp.where(at, 1.0, 0.0))
                mixing.append(jnp.where(at, jnp.broadcast_to(weights[j:j + 1, :], (items, tok_rows)), 0.0))
            picks = jnp.concatenate(chosen, axis=0).astype(jnp.bfloat16)
            outbound = jnp.dot(picks, block[source], preferred_element_type=jnp.float32).astype(jnp.bfloat16)
            for j in range(plane):
                picked[j, source] = outbound[j * items:(j + 1) * items]
            mix = jnp.concatenate(mixing, axis=0).T
            high = mix.astype(jnp.bfloat16)
            mix_high[source] = high
            mix_low[source] = (mix - high.astype(jnp.float32)).astype(jnp.bfloat16)
            return carry

        lax.fori_loop(0, depths, one, 0)
        for step in range(1, plane):
            peer = lax.rem(q + step, plane)
            remote(picked.at[peer], rows.at[core, q], p_sem.at[0], p_sem.at[1], fs(z * plane + peer))
        own_pick.start()

    swaps = []

    def collect():
        drain(rows.at[core, pl.ds(0, plane - 1)], p_sem.at[1])
        own_pick.wait()
        swaps.extend(swap(rows, 1))

    first = 2 * pieces
    tasks = {}
    for at, task in ((0, forward), (1, dispatch), (3, collect)):
        tasks.setdefault(min(at, first - 1), []).append(task)
    outs = []
    for index in range(first):
        arrive(index)
        for task in tasks.get(index, ()):
            task()
        if index == pieces - 1:
            outs.append(pltpu.make_async_copy(gate, gate_out, out_sem.at[0]))
            outs[-1].start()
        if index == first - 1:
            outs.append(pltpu.make_async_copy(up, up_out, out_sem.at[1]))
            outs[-1].start()
    for copy in swaps:
        copy.wait()

    tile = depths * items

    def first_layer(group, carry):
        gate_pre = jnp.zeros((tile, columns), jnp.float32)
        up_pre = jnp.zeros((tile, columns), jnp.float32)
        for part in range(cores):
            taken = rows[part, group].reshape(tile, width)
            span = pl.ds(part * width, width)
            gate_pre = gate_pre + jnp.dot(taken, gate[span, :], preferred_element_type=jnp.float32)
            up_pre = up_pre + jnp.dot(taken, up[span, :], preferred_element_type=jnp.float32)
        hidden[core, group] = activate(gate_pre, up_pre).astype(jnp.bfloat16)
        return carry

    lax.fori_loop(0, plane, first_layer, 0)
    for copy in swap(hidden, 2):
        copy.wait()

    def expert(c):
        arrive(first + c)
        outs.append(pltpu.make_async_copy(down.at[c], down_out.at[:, pl.ds(c * chunk, chunk)], out_sem.at[2 + c]))
        outs[-1].start()

        def second_layer(group):
            summed = jnp.zeros((tile, chunk), jnp.float32)
            for part in range(cores):
                summed = summed + jnp.dot(
                    hidden[part, group], down[c, pl.ds(part * columns, columns), :], preferred_element_type=jnp.float32
                )
            return summed.astype(jnp.bfloat16).reshape(depths, items, chunk)

        def one(step, carry):
            peer = lax.rem(q + step, plane)
            results[c, peer] = second_layer(peer)
            remote(results.at[c, peer], back.at[c, q], r_send.at[c], r_recv.at[c], fs(z * plane + peer))
            return carry

        lax.fori_loop(1, plane, one, 0)
        back[c, q] = second_layer(q)

    def relay(c):
        drain(back.at[c, pl.ds(0, plane - 1)], r_recv.at[c])

        def one(step, carry):
            target = lax.rem(z + 1 + step, depths)
            data = back[c, :, target].reshape(plane * items, chunk)
            summed = jnp.dot(mix_high[target], data, preferred_element_type=jnp.float32)
            summed = summed + jnp.dot(mix_low[target], data, preferred_element_type=jnp.float32)
            part_f[c, target] = summed
            part_s[c, target] = summed.astype(jnp.bfloat16)
            return carry

        lax.fori_loop(0, depths, one, 0)

        @pl.when(z != leader)
        def _():
            remote(
                part_s.at[c, pl.ds(other, half)], lead_in.at[c, place_in_half],
                l_send.at[c], l_recv.at[c], fs(leader * plane + q),
            )

        for step in range(1, half):
            target = base + lax.rem(place_in_half + step, half)
            remote(
                part_s.at[c, target], half_in.at[c, place_in_half],
                h_send.at[c], h_recv.at[c], fs(target * plane + q),
            )

    def lead(c):
        @pl.when(z == leader)
        def _():
            if half > 1:
                drain(lead_in.at[c, pl.ds(0, half - 1)], l_recv.at[c])
            for k in range(half):
                summed = part_f[c, other + k]
                for step in range(1, half):
                    summed = summed + lead_in[c, lax.rem(place_in_half + step, half), k].astype(jnp.float32)
                cross[c, k] = summed.astype(jnp.bfloat16)
            for k in range(half):
                remote(cross.at[c, k], cross_in.at[c], x_send.at[c], x_recv.at[c], fs((other + k) * plane + q))

    def finish(c):
        summed = part_f[c, z]
        if half > 1:
            drain(half_in.at[c, pl.ds(0, half - 1)], h_recv.at[c])
            for step in range(1, half):
                summed = summed + half_in[c, lax.rem(place_in_half + step, half)].astype(jnp.float32)
        drain(cross_in.at[c], x_recv.at[c])
        summed = summed + cross_in[c].astype(jnp.float32)
        mixed[:, c * chunk:(c + 1) * chunk] = summed.astype(jnp.bfloat16)

    expert(0)
    for c in range(1, chunks):
        relay(c - 1)
        lead(c - 1)
        expert(c)
        finish(c - 1)
    relay(chunks - 1)
    lead(chunks - 1)
    finish(chunks - 1)
    last = pltpu.make_async_copy(mixed, mixed_out, out_sem.at[2 + chunks])
    last.start()

    for index, phase in enumerate(phases):
        _, _, sent, _, _, _, _, _ = phase
        drain(sent.at[pl.ds(0, n - 1)], w_send.at[index])
    drain(block.at[pl.ds(0, half)], t_send.at[0])
    drain(info.at[pl.ds(0, half)], t_send.at[1])
    drain(picked.at[pl.ds(0, plane - 1)], p_sem.at[0])
    for c in range(chunks):
        drain(results.at[c, pl.ds(0, plane - 1)], r_send.at[c])
        if half > 1:
            drain(part_s.at[c, pl.ds(0, half - 1)], h_send.at[c])

    @pl.when(z == leader)
    def _():
        for step in range(1, half):
            drain(block.at[pl.ds(0, half)], fwd_send.at[0])
            drain(info.at[pl.ds(0, half)], fwd_send.at[1])
        for c in range(chunks):
            drain(cross.at[c], x_send.at[c])

    @pl.when(z != leader)
    def _():
        for c in range(chunks):
            drain(part_s.at[c, pl.ds(0, half)], l_send.at[c])

    for copy in outs:
        copy.wait()
    last.wait()


def shards(n, cores, tokens, norm_gain, gate_weight, up_weight, down_weight, routes, route_weights):
    experts, depth, columns = gate_weight.shape
    units, width = down_weight.shape[1:]
    tok_rows, top_count = routes.shape
    items = 2 * tok_rows * top_count // experts
    plane = plane_size(n)
    depths = n // plane
    half = depths // 2
    pieces = max(1, min(PIECES, depth // 32))
    piece = depth // pieces
    chunk = max(128, width // CHUNKS)
    chunks = width // chunk
    lanes = min(128, width)
    bf16, f32, dma = jnp.bfloat16, jnp.float32, pltpu.SemaphoreType.DMA
    phases = 2 * pieces + chunks

    anywhere = pl.BlockSpec(memory_space=pl.ANY)
    mixed, gate_ready, up_ready, down_ready = pl.pallas_call(
        functools.partial(kernel, n, cores, items, pieces, chunks),
        out_shape=(
            jax.ShapeDtypeStruct((tok_rows, width), bf16),
            jax.ShapeDtypeStruct((n * depth, columns), bf16),
            jax.ShapeDtypeStruct((n * depth, columns), bf16),
            jax.ShapeDtypeStruct((n * units, width), bf16),
        ),
        in_specs=[anywhere] * 7,
        out_specs=(anywhere,) * 4,
        scratch_shapes=[
            pltpu.VMEM((tok_rows, width), bf16),
            pltpu.VMEM((1, depth), f32),
            pltpu.VMEM((depth, lanes), f32),
            pltpu.VMEM((top_count, tok_rows), jnp.int32),
            pltpu.VMEM((top_count, tok_rows), f32),
            pltpu.VMEM((cores, tok_rows, lanes), f32),
            pltpu.VMEM((pieces, n, piece, columns), f32),
            pltpu.VMEM((pieces, n, piece, columns), f32),
            pltpu.VMEM((chunks, n, units, chunk), f32),
            pltpu.VMEM((pieces, n, piece, columns), bf16),
            pltpu.VMEM((pieces, n, piece, columns), bf16),
            pltpu.VMEM((chunks, n, units, chunk), bf16),
            pltpu.VMEM((n * depth, columns), bf16),
            pltpu.VMEM((n * depth, columns), bf16),
            pltpu.VMEM((chunks, n * units, chunk), bf16),
            pltpu.VMEM((depths, tok_rows, width), bf16),
            pltpu.VMEM((depths, 2, depths, plane, tok_rows), f32),
            pltpu.VMEM((depths, tok_rows, plane * items), bf16),
            pltpu.VMEM((depths, tok_rows, plane * items), bf16),
            pltpu.VMEM((plane, depths, items, width), bf16),
            pltpu.VMEM((cores, plane, depths, items, width), bf16),
            pltpu.VMEM((cores, plane, depths * items, columns), bf16),
            pltpu.VMEM((chunks, plane, depths, items, chunk), bf16),
            pltpu.VMEM((chunks, plane, depths, items, chunk), bf16),
            pltpu.VMEM((chunks, depths, tok_rows, chunk), f32),
            pltpu.VMEM((chunks, depths, tok_rows, chunk), bf16),
            pltpu.VMEM((chunks, half, half, tok_rows, chunk), bf16),
            pltpu.VMEM((chunks, half, tok_rows, chunk), bf16),
            pltpu.VMEM((chunks, half, tok_rows, chunk), bf16),
            pltpu.VMEM((chunks, tok_rows, chunk), bf16),
            pltpu.VMEM((tok_rows, width), bf16),
            dma((4 + phases,)),
            dma((phases,)),
            dma((phases,)),
            dma((2,)),
            dma((2,)),
            dma((2,)),
            dma((2,)),
            dma((3,)),
            dma((3, max(1, cores - 1))),
            dma((3, max(1, cores - 1))),
            dma((chunks,)),
            dma((chunks,)),
            dma((chunks,)),
            dma((chunks,)),
            dma((chunks,)),
            dma((chunks,)),
            dma((chunks,)),
            dma((chunks,)),
            dma((3 + chunks,)),
        ],
        compiler_params=pltpu.CompilerParams(
            collective_id=0, has_side_effects=True, vmem_limit_bytes=58 * 1024 * 1024
        ),
    )(tokens, norm_gain.reshape(1, depth), gate_weight, up_weight, down_weight, routes.T, route_weights.T)
    return (mixed, gate_ready[None], up_ready[None], down_ready[None])


def solution(mesh):
    placed = (
        P("fs", "tp"),
        P("fs"),
        P(None, "fs", "tp"),
        P(None, "fs", "tp"),
        P(None, "fs", "tp"),
        P("fs", None),
        P("fs", None),
    )
    return jax.shard_map(
        functools.partial(shards, mesh.shape["fs"], mesh.shape["tp"]),
        mesh=mesh,
        in_specs=placed,
        out_specs=(P("fs", "tp"), P("fs", None, "tp"), P("fs", None, "tp"), P("fs", None, "tp")),
        check_vma=False,
    )
```

time: 270 us -> 197 us (0.73)
  the two profiles are of different devices: /device:TPU:20 before, /device:TPU:0 now
where the time goes in v1:
time: 197 us; the launch traced here: 196 us
  Pallas kernels  187 us (95%)
  local copies, waits for them, and re-layouts  8.53 us (4%)
    pallas_call x1, Pallas kernels, shards(): pl.pallas_call(functools.partial(kernel, n, cores, items, pieces, chunks)...  187 us
    unnamed x8, local copies, waits for them, and re-layouts  8.53 us

profile of v1, /device:TPU:0, one launch (start us, length us, event | category | flops | bytes accessed | tf_op | source)
XLA Modules:
  0.0 196.1 jit_solution(3911781272563169428)
XLA Ops:
  0.6 186.9 %shard_map.102 = (bf16[128,1024]{1,0:T(8,128)(2,1)}, bf16[2048,512]{1,0:T(8,128)(2,1)}, bf16[2048,512]{1,0:T(8,128)(2,1)}, bf16[1024,1024]{1,0:T(8,128)(2,1)}) custom-call(bf16[128,1024]{1,0:T(8,128)(2,1)} %tokens_in.1, f32[1,128]{1,0:T(1,128)} %bitcast.11, f32[16,128,512]{2,1,0:T(8,128)} %gate_in.1, f32[16,128,512]{2,1,0:T(8,128)} %up_in.1, ...), custom_call_target="tpu_custom_call" | custom-call | tf_op jit(solution)/shard_map/pallas_call | solution.py:435
  187.5 1.7 copy.15
  189.2 0.0 copy-start.1
  189.2 3.2 %copy.16 = bf16[1,2048,512]{2,1,0:T(8,128)(2,1)} copy(bf16[1,2048,512]{2,1,0:T(8,128)(2,1)} %bitcast.8) | data formatting | bytes 4194304
  192.4 0.0 copy-done.1
  192.4 0.0 copy-start
  192.4 1.3 copy.17
  193.7 1.0 copy-done
  194.8 1.3 copy.18
Async XLA Ops:
  189.2 3.2 %copy-start.1 = (bf16[2048,512]{1,0:T(8,128)(2,1)S(1)}, bf16[2048,512]{1,0:T(8,128)(2,1)}, u32[]{:S(2)}) copy-start(bf16[2048,512]{1,0:T(8,128)(2,1)} %get-tuple-element.10) | copy-start | bytes 6291460
  192.4 2.3 %copy-start = (bf16[1024,1024]{1,0:T(8,128)(2,1)S(1)}, bf16[1024,1024]{1,0:T(8,128)(2,1)}, u32[]{:S(2)}) copy-start(bf16[1024,1024]{1,0:T(8,128)(2,1)} %get-tuple-element.11) | copy-start | bytes 6291460

commit v2 on v1

v2 whole, which is shorter than its diff:
```python
import functools
import math

import jax
import jax.numpy as jnp
from jax import lax
from jax.experimental import pallas as pl
from jax.experimental.pallas import tpu as pltpu
from jax.sharding import PartitionSpec as P

epsilon = 1e-05
MESH = pl.DeviceIdType.MESH
CHUNKS = 8
PARTS = 4
WINDOW, LATE_WINDOW = 4, 3
RELAY_LAG, LEAD_LAG, END_LAG = 4, 6, 7
NEAR_AT, FORWARD_AT, FAR_AT, COLLECT_AT = 2, 2, 7, 12


def activate(gate_pre, up_pre):
    gated = jnp.minimum(gate_pre, 7.0)
    upper = jnp.clip(up_pre, -7.0, 7.0)
    return (upper + 1.0) * gated * jax.nn.sigmoid(1.702 * gated)


def plane_size(n):
    return max(size for size in range(1, math.isqrt(n) + 1) if n % size == 0 and (n // size) % 2 == 0)


def kernel(
    n, cores, items, parts, chunks,
    tokens_in, gain_in, gate_in, up_in, down_in, routes_in, weights_in,
    mixed, pair, down,
    tok_raw, gain_row, gain_tile, routes_v, weights_v, square,
    gate_f, up_f, down_f, pair_s, down_s,
    block, info, picks, mix_high, mix_low, picked, rows, hidden,
    results, back, part_f, part_s, lead_in, half_in, cross, cross_in,
    load_sem, w_send, w_recv, t_send, near_recv, far_recv, fwd_send, p_send, p_recv, own_sem, tp_send, tp_recv,
    r_send, r_recv, h_send, h_recv, l_send, l_recv, x_send, x_recv,
):
    me = lax.axis_index("fs")
    core = lax.axis_index("tp")
    plane = plane_size(n)
    depths = n // plane
    half = depths // 2
    z = me // plane
    q = lax.rem(me, plane)
    base = (z // half) * half
    other = half - base
    leader = half - 1 + z // half
    other_leader = half - z // half
    place_in_half = z - base

    tok_rows, width = tokens_in.shape
    depth, columns = gate_in.shape[1:]
    units = down_in.shape[1]
    pieces = pair.shape[0]
    lanes = columns // pieces
    size = depth // parts
    chunk = width // chunks
    top_count = routes_in.shape[0]

    def fs(index):
        return {"fs": index}

    def remote(source, landing, sent, received, where):
        pltpu.make_async_remote_copy(
            src_ref=source, dst_ref=landing, send_sem=sent, recv_sem=received,
            device_id=where, device_id_type=MESH,
        ).start()

    def drain(ref, semaphore):
        pltpu.make_async_copy(ref, ref, semaphore).wait()

    barrier = pltpu.get_barrier_semaphore()

    def greet(step, carry):
        pl.semaphore_signal(barrier, inc=1, device_id=fs(lax.rem(me + step, n)), device_id_type=MESH)
        return carry

    lax.fori_loop(1, n, greet, 0)
    for step in range(1, cores):
        pl.semaphore_signal(barrier, inc=1, device_id={"tp": lax.rem(core + step, cores)}, device_id_type=MESH)

    small = ((tokens_in, tok_raw), (gain_in, gain_row), (routes_in, routes_v), (weights_in, weights_v))
    loads = [pltpu.make_async_copy(source, landing, load_sem.at[i, 0]) for i, (source, landing) in enumerate(small)]
    phases = []
    for p in range(pieces):
        for r in range(parts):
            at = pl.ds(r * size, size), pl.ds(p * lanes, lanes)
            sources = ((gate_in.at[:, at[0], at[1]], gate_f.at[p, r]), (up_in.at[:, at[0], at[1]], up_f.at[p, r]))
            phases.append((sources, pair_s.at[p, r], pair.at[p], depth, r * size, size))
    for c in range(chunks):
        sources = ((down_in.at[:, :, pl.ds(c * chunk, chunk)], down_f.at[c]),)
        phases.append((sources, down_s.at[c], down.at[c], units, 0, units))
    weight_loads = []
    for phase in phases:
        at = len(small) + len(weight_loads)
        weight_loads.append([
            pltpu.make_async_copy(source, landing, load_sem.at[at, i]) for i, (source, landing) in enumerate(phase[0])
        ])
    loads[1].start()
    for copy in weight_loads[0]:
        copy.start()
    for at in (0, 2, 3):
        loads[at].start()
    for copies in weight_loads[1:]:
        for copy in copies:
            copy.start()

    loads[1].wait()
    row_at = lax.broadcasted_iota(jnp.int32, (depth, depth), 0)
    lane_at = lax.broadcasted_iota(jnp.int32, (depth, depth), 1)
    spread = jnp.where(row_at == lane_at, jnp.broadcast_to(gain_row[...], (depth, depth)), 0.0)
    gain_tile[...] = jnp.broadcast_to(jnp.sum(spread, axis=1, keepdims=True), gain_tile.shape)

    def cast(index):
        sources, sent, landing, stride, offset, rows_sent = phases[index]
        for copy in weight_loads[index]:
            copy.wait()

        def rounded(peer):
            if len(sources) == 1:
                return sources[0][1][peer].astype(jnp.bfloat16)
            gain = gain_tile[offset:offset + rows_sent, :]
            return jnp.concatenate([(staged[peer] * gain).astype(jnp.bfloat16) for _, staged in sources], axis=1)

        def one(step, carry):
            peer = lax.rem(me + step, n)
            sent[peer] = rounded(peer)
            return carry

        lax.fori_loop(1, n, one, 0)
        landing[pl.ds(pl.multiple_of(me * stride + offset, rows_sent), rows_sent), :] = rounded(me)

    def send(index):
        _, sent, landing, stride, offset, rows_sent = phases[index]

        def one(step, carry):
            peer = lax.rem(me + step, n)
            remote(
                sent.at[peer], landing.at[pl.ds(pl.multiple_of(me * stride + offset, rows_sent), rows_sent)],
                w_send.at[index], w_recv.at[index], fs(peer),
            )
            return carry

        lax.fori_loop(1, n, one, 0)

    first = pieces * parts
    issued = []

    def arrive(index):
        _, _, landing, _, _, rows_sent = phases[index]
        drain(landing.at[pl.ds(0, (n - 1) * rows_sent)], w_recv.at[index])
        ahead = index + (WINDOW if index < first else LATE_WINDOW)
        while len(issued) <= min(ahead, len(phases) - 1):
            send(len(issued))
            issued.append(len(issued))

    def swap(buffer, slot):
        copies = []
        for step in range(1, cores):
            copies.append(
                pltpu.make_async_remote_copy(
                    src_ref=buffer, dst_ref=buffer,
                    send_sem=tp_send.at[slot, step - 1], recv_sem=tp_recv.at[slot, step - 1],
                    device_id={"tp": lax.rem(core + step, cores)}, device_id_type=MESH,
                )
            )
        for copy in copies:
            copy.start()
        return copies

    cast(0)
    loads[0].wait()
    values = tok_raw[...].astype(jnp.float32)
    square[core] = jnp.broadcast_to(jnp.sum(values * values, axis=1, keepdims=True), square.shape[1:])
    pl.semaphore_wait(barrier, n - 1 + cores - 1)
    send(0)
    issued.append(0)
    swapped = swap(square.at[core], 0)

    loads[2].wait()
    loads[3].wait()
    names = lax.broadcasted_iota(jnp.int32, (n, tok_rows), 0)
    weight = jnp.zeros((n, tok_rows), jnp.float32)
    member = jnp.zeros((n, tok_rows), jnp.float32)
    for k in range(top_count):
        hit = jnp.broadcast_to(routes_v[k:k + 1, :], (n, tok_rows)) == names
        weight = weight + jnp.where(hit, jnp.broadcast_to(weights_v[k:k + 1, :], (n, tok_rows)), 0.0)
        member = member + jnp.where(hit, 1.0, 0.0)
    before = lax.broadcasted_iota(jnp.int32, (tok_rows, tok_rows), 0)
    after = lax.broadcasted_iota(jnp.int32, (tok_rows, tok_rows), 1)
    earlier = jnp.where(before < after, 1.0, 0.0).astype(jnp.bfloat16)
    place = jnp.dot(member.astype(jnp.bfloat16), earlier, preferred_element_type=jnp.float32)
    place = jnp.where(member > 0.0, place, -1.0)
    for p in range(depths):
        info[z, 0, p] = weight[p * plane:(p + 1) * plane]
        info[z, 1, p] = place[p * plane:(p + 1) * plane]

    for copy in swapped:
        copy.wait()
    total = square[0]
    for part in range(1, cores):
        total = total + square[part]
    scale = lax.rsqrt(total / (width * cores) + epsilon)
    values = tok_raw[...].astype(jnp.float32)
    scale = jnp.concatenate([scale] * (width // scale.shape[1]), axis=1)
    block[z] = (values * scale).astype(jnp.bfloat16)

    def give_tokens(dest, received):
        remote(block.at[z], block.at[z], t_send.at[0], received.at[0], fs(dest * plane + q))
        remote(info.at[z], info.at[z], t_send.at[1], received.at[1], fs(dest * plane + q))

    give_tokens(other_leader, far_recv)
    for step in range(1, half):
        give_tokens(base + lax.rem(place_in_half + step, half), near_recv)
    for index in range(1, min(WINDOW, len(phases))):
        cast(index)
        send(index)
        issued.append(index)
    for index in range(WINDOW, len(phases)):
        cast(index)

    def take_far():
        drain(block.at[pl.ds(0, half)], far_recv.at[0])
        drain(info.at[pl.ds(0, half)], far_recv.at[1])

    def forward():
        @pl.when(z == leader)
        def _():
            take_far()
            for step in range(1, half):
                dest = fs((base + lax.rem(place_in_half + step, half)) * plane + q)
                remote(block.at[pl.ds(other, half)], block.at[pl.ds(other, half)], fwd_send.at[0], far_recv.at[0], dest)
                remote(info.at[pl.ds(other, half)], info.at[pl.ds(other, half)], fwd_send.at[1], far_recv.at[1], dest)

    slices = picked.shape[0]
    slice_width = width // slices
    own_picks = [
        pltpu.make_async_copy(picked.at[f, q], rows.at[core, f, q], own_sem.at[f]) for f in range(slices)
    ]

    def choose(source):
        slot = lax.broadcasted_iota(jnp.int32, (items, tok_rows), 0).astype(jnp.float32)
        weights = info[source, 0, z]
        places = info[source, 1, z]
        chosen, mixing = [], []
        for j in range(plane):
            at = jnp.broadcast_to(places[j:j + 1, :], (items, tok_rows)) == slot
            chosen.append(jnp.where(at, 1.0, 0.0))
            mixing.append(jnp.where(at, jnp.broadcast_to(weights[j:j + 1, :], (items, tok_rows)), 0.0))
        picks[...] = jnp.concatenate(chosen, axis=0).astype(jnp.bfloat16)
        mix = jnp.concatenate(mixing, axis=0).T
        high = mix.astype(jnp.bfloat16)
        mix_high[source] = high
        mix_low[source] = (mix - high.astype(jnp.float32)).astype(jnp.bfloat16)

    def dispatch(turn, f):
        if turn < half:
            source = base + lax.rem(place_in_half + turn, half)
        else:
            source = other + (turn - half)
        if f == 0:
            if turn == 1:
                drain(block.at[pl.ds(0, half - 1)], near_recv.at[0])
                drain(info.at[pl.ds(0, half - 1)], near_recv.at[1])
            if turn == half:
                @pl.when(z != leader)
                def _():
                    take_far()
            choose(source)
        part = block[source, :, f * slice_width:(f + 1) * slice_width]
        outbound = jnp.dot(picks[...], part, preferred_element_type=jnp.float32).astype(jnp.bfloat16)
        for j in range(plane):
            picked[f, j, source] = outbound[j * items:(j + 1) * items]
        for step in range(1, plane):
            peer = lax.rem(q + step, plane)
            remote(
                picked.at[f, peer, source], rows.at[core, f, q, source],
                p_send.at[f], p_recv.at[f], fs(z * plane + peer),
            )
        if turn == depths - 1:
            own_picks[f].start()

    swaps = []

    def collect():
        for f in range(slices):
            drain(rows.at[core, f, pl.ds(0, plane - 1)], p_recv.at[f])
            own_picks[f].wait()
        swaps.extend(swap(rows.at[core], 1))

    steps = [(0, dispatch, (0, 0))]
    for turn in range(depths):
        for f in range(slices):
            if turn + f > 0:
                at = turn * slices + f if turn < half else FAR_AT + (turn - half) * slices + f
                steps.append((at, dispatch, (turn, f)))
    at_far = next(i for i, (_, _, what) in enumerate(steps) if what[0] == half)
    steps.insert(at_far, (FORWARD_AT, forward, ()))
    steps.append((COLLECT_AT, collect, ()))
    tasks = {}
    for at, task, what in steps:
        tasks.setdefault(min(at, first - 1), []).append((task, what))
    tile = depths * items

    def first_layer(p):
        def one(group, carry):
            both = jnp.zeros((tile, 2 * lanes), jnp.float32)
            for part in range(cores):
                taken = jnp.concatenate([rows[part, f, group].reshape(tile, slice_width) for f in range(slices)], axis=1)
                both = both + jnp.dot(taken, pair[p, pl.ds(part * width, width), :], preferred_element_type=jnp.float32)
            hidden[core, p, group] = activate(both[:, :lanes], both[:, lanes:]).astype(jnp.bfloat16)
            return carry

        lax.fori_loop(0, plane, one, 0)
        swaps.extend(swap(hidden.at[core, p], 2 + p))

    computed = 0
    for index in range(first):
        arrive(index)
        for task, what in tasks.get(index, ()):
            task(*what)
        if index > COLLECT_AT or index == first - 1:
            if computed == 0:
                while swaps:
                    swaps.pop().wait()
            while (computed + 1) * parts <= index + 1:
                first_layer(computed)
                computed += 1

    def expert(c):
        arrive(first + c)
        while swaps:
            swaps.pop(0).wait()

        def second_layer(group):
            summed = jnp.zeros((tile, chunk), jnp.float32)
            for part in range(cores):
                units_in = jnp.concatenate([hidden[part, p, group] for p in range(pieces)], axis=1)
                summed = summed + jnp.dot(
                    units_in, down[c, pl.ds(part * columns, columns), :], preferred_element_type=jnp.float32
                )
            return summed.astype(jnp.bfloat16).reshape(depths, items, chunk)

        def one(step, carry):
            peer = lax.rem(q + step, plane)
            results[c, peer] = second_layer(peer)
            remote(results.at[c, peer], back.at[c, q], r_send.at[c], r_recv.at[c], fs(z * plane + peer))
            return carry

        lax.fori_loop(1, plane, one, 0)
        back[c, q] = second_layer(q)

    def relay(c):
        drain(back.at[c, pl.ds(0, plane - 1)], r_recv.at[c])

        def one(step, carry):
            target = lax.rem(z + 1 + step, depths)
            data = back[c, :, target].reshape(plane * items, chunk)
            summed = jnp.dot(mix_high[target], data, preferred_element_type=jnp.float32)
            summed = summed + jnp.dot(mix_low[target], data, preferred_element_type=jnp.float32)
            part_f[c, target] = summed
            part_s[c, target] = summed.astype(jnp.bfloat16)
            return carry

        lax.fori_loop(0, depths, one, 0)

        @pl.when(z != leader)
        def _():
            remote(
                part_s.at[c, pl.ds(other, half)], lead_in.at[c, place_in_half],
                l_send.at[c], l_recv.at[c], fs(leader * plane + q),
            )

        for step in range(1, half):
            target = base + lax.rem(place_in_half + step, half)
            remote(
                part_s.at[c, target], half_in.at[c, place_in_half],
                h_send.at[c], h_recv.at[c], fs(target * plane + q),
            )

    def lead(c):
        @pl.when(z == leader)
        def _():
            if half > 1:
                drain(lead_in.at[c, pl.ds(0, half - 1)], l_recv.at[c])
            for k in range(half):
                summed = part_f[c, other + k]
                for step in range(1, half):
                    summed = summed + lead_in[c, lax.rem(place_in_half + step, half), k].astype(jnp.float32)
                cross[c, k] = summed.astype(jnp.bfloat16)
            for k in range(half):
                remote(cross.at[c, k], cross_in.at[c], x_send.at[c], x_recv.at[c], fs((other + k) * plane + q))

    def finish(c):
        summed = part_f[c, z]
        if half > 1:
            drain(half_in.at[c, pl.ds(0, half - 1)], h_recv.at[c])
            for step in range(1, half):
                summed = summed + half_in[c, lax.rem(place_in_half + step, half)].astype(jnp.float32)
        drain(cross_in.at[c], x_recv.at[c])
        summed = summed + cross_in[c].astype(jnp.float32)
        mixed[:, c * chunk:(c + 1) * chunk] = summed.astype(jnp.bfloat16)

    stages = ((relay, RELAY_LAG), (lead, LEAD_LAG), (finish, END_LAG))
    done = [0, 0, 0]
    for c in range(chunks):
        expert(c)
        for stage, (task, lag) in enumerate(stages):
            if c >= lag:
                task(done[stage])
                done[stage] += 1
    while done[0] < chunks:
        relay(done[0])
        done[0] += 1
        if done[1] < done[0] - 1:
            lead(done[1])
            done[1] += 1
    for c in range(done[1], chunks):
        lead(c)
    for c in range(done[2], chunks):
        finish(c)
    for index, phase in enumerate(phases):
        drain(phase[1].at[pl.ds(0, n - 1)], w_send.at[index])
    drain(block.at[pl.ds(0, half)], t_send.at[0])
    drain(info.at[pl.ds(0, half)], t_send.at[1])
    for f in range(slices):
        drain(picked.at[f, pl.ds(0, plane - 1)], p_send.at[f])
    for c in range(chunks):
        drain(results.at[c, pl.ds(0, plane - 1)], r_send.at[c])
        if half > 1:
            drain(part_s.at[c, pl.ds(0, half - 1)], h_send.at[c])

    @pl.when(z == leader)
    def _():
        for step in range(1, half):
            drain(block.at[pl.ds(0, half)], fwd_send.at[0])
            drain(info.at[pl.ds(0, half)], fwd_send.at[1])
        for c in range(chunks):
            drain(cross.at[c], x_send.at[c])

    @pl.when(z != leader)
    def _():
        for c in range(chunks):
            drain(part_s.at[c, pl.ds(0, half)], l_send.at[c])


def place(mixed, pair, down, mixed_out, gate_out, up_out, down_out, sem):
    pieces, _, both = pair.shape
    chunks, _, chunk = down.shape
    lanes = both // 2
    moves = [(mixed, mixed_out)]
    for p in range(pieces):
        at = pl.ds(p * lanes, lanes)
        moves.append((pair.at[p, :, pl.ds(0, lanes)], gate_out.at[:, at]))
        moves.append((pair.at[p, :, pl.ds(lanes, lanes)], up_out.at[:, at]))
    for c in range(chunks):
        moves.append((down.at[c], down_out.at[:, pl.ds(c * chunk, chunk)]))
    copies = [pltpu.make_async_copy(source, landing, sem.at[i]) for i, (source, landing) in enumerate(moves)]
    for copy in copies:
        copy.start()
    for copy in copies:
        copy.wait()


def shards(n, cores, tokens, norm_gain, gate_weight, up_weight, down_weight, routes, route_weights):
    experts, depth, columns = gate_weight.shape
    units, width = down_weight.shape[1:]
    tok_rows, top_count = routes.shape
    items = 2 * tok_rows * top_count // experts
    plane = plane_size(n)
    depths = n // plane
    half = depths // 2
    parts = max(1, min(PARTS, depth // 16))
    lanes = min(128, columns)
    pieces = columns // lanes
    chunk = max(128, width // CHUNKS)
    chunks = width // chunk
    slices = 2 if width % 256 == 0 else 1
    bf16, f32, dma = jnp.bfloat16, jnp.float32, pltpu.SemaphoreType.DMA
    phases = pieces * parts + chunks

    arrays = tokens, norm_gain.reshape(1, depth), gate_weight, up_weight, down_weight, routes.T, route_weights.T
    anywhere = pl.BlockSpec(memory_space=pl.ANY)
    near = pl.BlockSpec(memory_space=pltpu.VMEM)
    results = pl.pallas_call(
        functools.partial(kernel, n, cores, items, parts, chunks),
        out_shape=(
            jax.ShapeDtypeStruct((tok_rows, width), bf16),
            jax.ShapeDtypeStruct((pieces, n * depth, 2 * lanes), bf16),
            jax.ShapeDtypeStruct((chunks, n * units, chunk), bf16),
        ),
        in_specs=[anywhere] * 7,
        out_specs=(near,) * 3,
        scratch_shapes=[
            pltpu.VMEM((tok_rows, width), bf16),
            pltpu.VMEM((1, depth), f32),
            pltpu.VMEM((depth, lanes), f32),
            pltpu.VMEM((top_count, tok_rows), jnp.int32),
            pltpu.VMEM((top_count, tok_rows), f32),
            pltpu.VMEM((cores, tok_rows, lanes), f32),
            pltpu.VMEM((pieces, parts, n, depth // parts, lanes), f32),
            pltpu.VMEM((pieces, parts, n, depth // parts, lanes), f32),
            pltpu.VMEM((chunks, n, units, chunk), f32),
            pltpu.VMEM((pieces, parts, n, depth // parts, 2 * lanes), bf16),
            pltpu.VMEM((chunks, n, units, chunk), bf16),
            pltpu.VMEM((depths, tok_rows, width), bf16),
            pltpu.VMEM((depths, 2, depths, plane, tok_rows), f32),
            pltpu.VMEM((plane * items, tok_rows), bf16),
            pltpu.VMEM((depths, tok_rows, plane * items), bf16),
            pltpu.VMEM((depths, tok_rows, plane * items), bf16),
            pltpu.VMEM((slices, plane, depths, items, width // slices), bf16),
            pltpu.VMEM((cores, slices, plane, depths, items, width // slices), bf16),
            pltpu.VMEM((cores, pieces, plane, depths * items, lanes), bf16),
            pltpu.VMEM((chunks, plane, depths, items, chunk), bf16),
            pltpu.VMEM((chunks, plane, depths, items, chunk), bf16),
            pltpu.VMEM((chunks, depths, tok_rows, chunk), f32),
            pltpu.VMEM((chunks, depths, tok_rows, chunk), bf16),
            pltpu.VMEM((chunks, half, half, tok_rows, chunk), bf16),
            pltpu.VMEM((chunks, half, tok_rows, chunk), bf16),
            pltpu.VMEM((chunks, half, tok_rows, chunk), bf16),
            pltpu.VMEM((chunks, tok_rows, chunk), bf16),
            dma((4 + phases, 2)),
            dma((phases,)),
            dma((phases,)),
            dma((2,)),
            dma((2,)),
            dma((2,)),
            dma((2,)),
            dma((slices,)),
            dma((slices,)),
            dma((slices,)),
            dma((2 + pieces, max(1, cores - 1))),
            dma((2 + pieces, max(1, cores - 1))),
            dma((chunks,)),
            dma((chunks,)),
            dma((chunks,)),
            dma((chunks,)),
            dma((chunks,)),
            dma((chunks,)),
            dma((chunks,)),
            dma((chunks,)),
        ],
        compiler_params=pltpu.CompilerParams(
            collective_id=0, has_side_effects=True, vmem_limit_bytes=44 * 1024 * 1024
        ),
    )(*(pltpu.with_memory_space_constraint(array, pltpu.HBM) for array in arrays))
    ready = (tok_rows, width), (n * depth, columns), (n * depth, columns), (n * units, width)
    mixed, gate_ready, up_ready, down_ready = pl.pallas_call(
        place,
        out_shape=tuple(jax.ShapeDtypeStruct(shape, bf16) for shape in ready),
        in_specs=[anywhere] * 3,
        out_specs=(anywhere,) * 4,
        scratch_shapes=[dma((1 + 2 * pieces + chunks,))],
        compiler_params=pltpu.CompilerParams(vmem_limit_bytes=1024 * 1024),
    )(*results)
    return (mixed, gate_ready[None], up_ready[None], down_ready[None])


def solution(mesh):
    placed = (
        P("fs", "tp"),
        P("fs"),
        P(None, "fs", "tp"),
        P(None, "fs", "tp"),
        P(None, "fs", "tp"),
        P("fs", None),
        P("fs", None),
    )
    return jax.shard_map(
        functools.partial(shards, mesh.shape["fs"], mesh.shape["tp"]),
        mesh=mesh,
        in_specs=placed,
        out_specs=(P("fs", "tp"), P("fs", None, "tp"), P("fs", None, "tp"), P("fs", None, "tp")),
        check_vma=False,
    )
```

time: 197 us -> 177 us (0.90)
  Pallas kernels: 187 us -> 176 us
  local copies, waits for them, and re-layouts: 8.53 us -> 0 us
    pallas_call x1 -> x2, Pallas kernels: 187 us -> 176 us  [the longest x1 174 us: shards(): pl.pallas_call(functools.partial(kernel, n, cores, items, parts, chunks),...]
    unnamed x8 -> x0, local copies, waits for them, and re-layouts: 8.53 us -> none
where the time goes in v2:
time: 177 us
  Pallas kernels  176 us (99%)
    pallas_call x1, Pallas kernels, shards(): pl.pallas_call(functools.partial(kernel, n, cores, items, parts, chunks),...  174 us

profile of v2, /device:TPU:0, one launch (start us, length us, event | category | flops | bytes accessed | tf_op | source)
XLA Modules:
  0.0 177.0 jit_solution(15946217523166313424)
XLA Ops:
  0.6 173.5 %shard_map.102 = (bf16[128,1024]{1,0:T(8,128)(2,1)S(1)}, bf16[4,2048,256]{2,1,0:T(8,128)(2,1)S(1)}, bf16[8,1024,128]{2,1,0:T(8,128)(2,1)S(1)}) custom-call(bf16[128,1024]{1,0:T(8,128)(2,1)} %tokens_in.1, f32[1,128]{1,0:T(1,128)} %bitcast.8, f32[16,128,512]{2,1,0:T(8,128)} %gate_in.1, f32[16,128,512]{2,1,0:T(8,128)} %up_in.1, f32[16,64,1024]{2,1,0:T(8,128)} %down_in.1, ...), custom_call_target="tpu_custom_call" | custom-call | tf_op jit(solution)/shard_map/pallas_call | solution.py:488
  174.1 2.9 %shard_map.103 = (bf16[128,1024]{1,0:T(8,128)(2,1)}, bf16[2048,512]{1,0:T(8,128)(2,1)}, bf16[2048,512]{1,0:T(8,128)(2,1)}, bf16[1024,1024]{1,0:T(8,128)(2,1)}) custom-call(bf16[128,1024]{1,0:T(8,128)(2,1)S(1)} %get-tuple-element.11.mixed, bf16[4,2048,256]{2,1,0:T(8,128)(2,1)S(1)} %get-tuple-element.12.pair, bf16[8,1024,128]{2,1,0:T(8,128)(2,1)S(1)} %get-tuple-element.13.down), custom_call_target="tpu_custom_call" | custom-call | tf_op jit(solution)/shard_map/pallas_call | solution.py:551

commit v3 on v2

--- a/solution.py
+++ b/solution.py
@@ -13,7 +13,8 @@
 CHUNKS = 8
 PARTS = 4
 WINDOW, LATE_WINDOW = 4, 3
-RELAY_LAG, LEAD_LAG, END_LAG = 4, 6, 7
+RELAY_LAG, LEAD_LAG, END_LAG = 2, 4, 7
+DIRECT = 1
 NEAR_AT, FORWARD_AT, FAR_AT, COLLECT_AT = 2, 2, 7, 12
 
 
@@ -330,6 +331,9 @@
                 first_layer(computed)
                 computed += 1
 
+    def direct(c):
+        return c >= chunks - DIRECT
+
     def expert(c):
         arrive(first + c)
         while swaps:
@@ -344,36 +348,62 @@
                 )
             return summed.astype(jnp.bfloat16).reshape(depths, items, chunk)
 
-        def one(step, carry):
+        def give(peer, start, which):
+            at = pl.ds(start, half)
+            remote(
+                results.at[c, peer, at], back.at[c, q, at],
+                r_send.at[c, which], r_recv.at[c, which], fs(z * plane + peer),
+            )
+
+        def far(step, carry):
             peer = lax.rem(q + step, plane)
             results[c, peer] = second_layer(peer)
-            remote(results.at[c, peer], back.at[c, q], r_send.at[c], r_recv.at[c], fs(z * plane + peer))
+            give(peer, other, 0)
             return carry
 
-        lax.fori_loop(1, plane, one, 0)
+        def near(step, carry):
+            give(lax.rem(q + step, plane), base, 1)
+            return carry
+
+        lax.fori_loop(1, plane, far, 0)
+        lax.fori_loop(1, plane, near, 0)
         back[c, q] = second_layer(q)
 
     def relay(c):
-        drain(back.at[c, pl.ds(0, plane - 1)], r_recv.at[c])
-
-        def one(step, carry):
-            target = lax.rem(z + 1 + step, depths)
+        def mix(target):
             data = back[c, :, target].reshape(plane * items, chunk)
             summed = jnp.dot(mix_high[target], data, preferred_element_type=jnp.float32)
             summed = summed + jnp.dot(mix_low[target], data, preferred_element_type=jnp.float32)
             part_f[c, target] = summed
             part_s[c, target] = summed.astype(jnp.bfloat16)
+
+        def far(k, carry):
+            mix(other + k)
             return carry
 
-        lax.fori_loop(0, depths, one, 0)
-
-        @pl.when(z != leader)
-        def _():
-            remote(
-                part_s.at[c, pl.ds(other, half)], lead_in.at[c, place_in_half],
-                l_send.at[c], l_recv.at[c], fs(leader * plane + q),
-            )
-
+        def near(k, carry):
+            mix(base + lax.rem(place_in_half + k, half))
+            return carry
+
+        drain(back.at[c, pl.ds(0, plane - 1), pl.ds(0, half)], r_recv.at[c, 0])
+        lax.fori_loop(0, half, far, 0)
+
+        if direct(c):
+            for k in range(half):
+                remote(
+                    part_s.at[c, other + k], cross_in.at[c, place_in_half],
+                    x_send.at[c], x_recv.at[c], fs((other + k) * plane + q),
+                )
+        else:
+            @pl.when(z != leader)
+            def _():
+                remote(
+                    part_s.at[c, pl.ds(other, half)], lead_in.at[c, place_in_half],
+                    l_send.at[c], l_recv.at[c], fs(leader * plane + q),
+                )
+
+        drain(back.at[c, pl.ds(0, plane - 1), pl.ds(0, half)], r_recv.at[c, 1])
+        lax.fori_loop(0, half, near, 0)
         for step in range(1, half):
             target = base + lax.rem(place_in_half + step, half)
             remote(
@@ -382,6 +412,9 @@
             )
 
     def lead(c):
+        if direct(c):
+            return
+
         @pl.when(z == leader)
         def _():
             if half > 1:
@@ -392,7 +425,7 @@
                     summed = summed + lead_in[c, lax.rem(place_in_half + step, half), k].astype(jnp.float32)
                 cross[c, k] = summed.astype(jnp.bfloat16)
             for k in range(half):
-                remote(cross.at[c, k], cross_in.at[c], x_send.at[c], x_recv.at[c], fs((other + k) * plane + q))
+                remote(cross.at[c, k], cross_in.at[c, 0], x_send.at[c], x_recv.at[c], fs((other + k) * plane + q))
 
     def finish(c):
         summed = part_f[c, z]
@@ -400,8 +433,10 @@
             drain(half_in.at[c, pl.ds(0, half - 1)], h_recv.at[c])
             for step in range(1, half):
                 summed = summed + half_in[c, lax.rem(place_in_half + step, half)].astype(jnp.float32)
-        drain(cross_in.at[c], x_recv.at[c])
-        summed = summed + cross_in[c].astype(jnp.float32)
+        taken = half if direct(c) else 1
+        drain(cross_in.at[c, pl.ds(0, taken)], x_recv.at[c])
+        for k in range(taken):
+            summed = summed + cross_in[c, k].astype(jnp.float32)
         mixed[:, c * chunk:(c + 1) * chunk] = summed.astype(jnp.bfloat16)
 
     stages = ((relay, RELAY_LAG), (lead, LEAD_LAG), (finish, END_LAG))
@@ -412,6 +447,19 @@
             if c >= lag:
                 task(done[stage])
                 done[stage] += 1
+    for index, phase in enumerate(phases):
+        drain(phase[1].at[pl.ds(0, n - 1)], w_send.at[index])
+    drain(block.at[pl.ds(0, half)], t_send.at[0])
+    drain(info.at[pl.ds(0, half)], t_send.at[1])
+    for f in range(slices):
+        drain(picked.at[f, pl.ds(0, plane - 1)], p_send.at[f])
+
+    @pl.when(z == leader)
+    def _():
+        for step in range(1, half):
+            drain(block.at[pl.ds(0, half)], fwd_send.at[0])
+            drain(info.at[pl.ds(0, half)], fwd_send.at[1])
+
     while done[0] < chunks:
         relay(done[0])
         done[0] += 1
@@ -420,31 +468,29 @@
             done[1] += 1
     for c in range(done[1], chunks):
         lead(c)
-    for c in range(done[2], chunks):
-        finish(c)
-    for index, phase in enumerate(phases):
-        drain(phase[1].at[pl.ds(0, n - 1)], w_send.at[index])
-    drain(block.at[pl.ds(0, half)], t_send.at[0])
-    drain(info.at[pl.ds(0, half)], t_send.at[1])
-    for f in range(slices):
-        drain(picked.at[f, pl.ds(0, plane - 1)], p_send.at[f])
+
     for c in range(chunks):
-        drain(results.at[c, pl.ds(0, plane - 1)], r_send.at[c])
+        for which in range(2):
+            drain(results.at[c, pl.ds(0, plane - 1), pl.ds(0, half)], r_send.at[c, which])
         if half > 1:
             drain(part_s.at[c, pl.ds(0, half - 1)], h_send.at[c])
+        if direct(c):
+            drain(part_s.at[c, pl.ds(0, half)], x_send.at[c])
 
     @pl.when(z == leader)
     def _():
-        for step in range(1, half):
-            drain(block.at[pl.ds(0, half)], fwd_send.at[0])
-            drain(info.at[pl.ds(0, half)], fwd_send.at[1])
         for c in range(chunks):
-            drain(cross.at[c], x_send.at[c])
+            if not direct(c):
+                drain(cross.at[c], x_send.at[c])
 
     @pl.when(z != leader)
     def _():
         for c in range(chunks):
-            drain(part_s.at[c, pl.ds(0, half)], l_send.at[c])
+            if not direct(c):
+                drain(part_s.at[c, pl.ds(0, half)], l_send.at[c])
+
+    for c in range(done[2], chunks):
+        finish(c)
 
 
 def place(mixed, pair, down, mixed_out, gate_out, up_out, down_out, sem):
@@ -521,7 +567,7 @@
             pltpu.VMEM((chunks, half, half, tok_rows, chunk), bf16),
             pltpu.VMEM((chunks, half, tok_rows, chunk), bf16),
             pltpu.VMEM((chunks, half, tok_rows, chunk), bf16),
-            pltpu.VMEM((chunks, tok_rows, chunk), bf16),
+            pltpu.VMEM((chunks, half, tok_rows, chunk), bf16),
             dma((4 + phases, 2)),
             dma((phases,)),
             dma((phases,)),
@@ -534,8 +580,8 @@
             dma((slices,)),
             dma((2 + pieces, max(1, cores - 1))),
             dma((2 + pieces, max(1, cores - 1))),
-            dma((chunks,)),
-            dma((chunks,)),
+            dma((chunks, 2)),
+            dma((chunks, 2)),
             dma((chunks,)),
             dma((chunks,)),
             dma((chunks,)),

time: 177 us -> 173 us (0.977)
  Pallas kernels: 176 us -> 172 us
    pallas_call x1, Pallas kernels: 174 us -> 170 us  [shards(): pl.pallas_call(functools.partial(kernel, n, cores, items, parts, chunks),...]
where the time goes in v3:
time: 173 us
  Pallas kernels  172 us (99%)
    pallas_call x1, Pallas kernels, shards(): pl.pallas_call(functools.partial(kernel, n, cores, items, parts, chunks),...  170 us

profile of v3, /device:TPU:0, one launch (start us, length us, event | category | flops | bytes accessed | tf_op | source)
XLA Modules:
  0.0 173.1 jit_solution(17613288194788948438)
XLA Ops:
  0.6 169.6 %shard_map.102 = (bf16[128,1024]{1,0:T(8,128)(2,1)S(1)}, bf16[4,2048,256]{2,1,0:T(8,128)(2,1)S(1)}, bf16[8,1024,128]{2,1,0:T(8,128)(2,1)S(1)}) custom-call(bf16[128,1024]{1,0:T(8,128)(2,1)} %tokens_in.1, f32[1,128]{1,0:T(1,128)} %bitcast.8, f32[16,128,512]{2,1,0:T(8,128)} %gate_in.1, f32[16,128,512]{2,1,0:T(8,128)} %up_in.1, f32[16,64,1024]{2,1,0:T(8,128)} %down_in.1, ...), custom_call_target="tpu_custom_call" | custom-call | tf_op jit(solution)/shard_map/pallas_call | solution.py:534
  170.2 2.9 %shard_map.103 = (bf16[128,1024]{1,0:T(8,128)(2,1)}, bf16[2048,512]{1,0:T(8,128)(2,1)}, bf16[2048,512]{1,0:T(8,128)(2,1)}, bf16[1024,1024]{1,0:T(8,128)(2,1)}) custom-call(bf16[128,1024]{1,0:T(8,128)(2,1)S(1)} %get-tuple-element.11.mixed, bf16[4,2048,256]{2,1,0:T(8,128)(2,1)S(1)} %get-tuple-element.12.pair, bf16[8,1024,128]{2,1,0:T(8,128)(2,1)S(1)} %get-tuple-element.13.down), custom_call_target="tpu_custom_call" | custom-call | tf_op jit(solution)/shard_map/pallas_call | solution.py:597

commit v4 on v3

--- a/solution.py
+++ b/solution.py
@@ -12,9 +12,10 @@
 MESH = pl.DeviceIdType.MESH
 CHUNKS = 8
 PARTS = 4
-WINDOW, LATE_WINDOW = 4, 3
+WINDOW, LATE_WINDOW = 4, 4
 RELAY_LAG, LEAD_LAG, END_LAG = 2, 4, 7
 DIRECT = 1
+EARLY_AT = 5
 NEAR_AT, FORWARD_AT, FAR_AT, COLLECT_AT = 2, 2, 7, 12
 
 
@@ -134,20 +135,36 @@
         lax.fori_loop(1, n, one, 0)
         landing[pl.ds(pl.multiple_of(me * stride + offset, rows_sent), rows_sent), :] = rounded(me)
 
+    first = pieces * parts
+
     def send(index):
         _, sent, landing, stride, offset, rows_sent = phases[index]
 
-        def one(step, carry):
-            peer = lax.rem(me + step, n)
-            remote(
-                sent.at[peer], landing.at[pl.ds(pl.multiple_of(me * stride + offset, rows_sent), rows_sent)],
-                w_send.at[index], w_recv.at[index], fs(peer),
-            )
-            return carry
-
-        lax.fori_loop(1, n, one, 0)
-
-    first = pieces * parts
+        def to(peer, landing, sent, which, at):
+            remote(sent.at[peer], landing.at[at], w_send.at[which], w_recv.at[which], fs(peer))
+
+        def whole(step, carry):
+            at = pl.ds(pl.multiple_of(me * stride + offset, rows_sent), rows_sent)
+            to(lax.rem(me + step, n), landing, sent, index, at)
+            return carry
+
+        def beyond(step, carry):
+            at = pl.ds(pl.multiple_of(me * stride + offset, rows_sent), rows_sent)
+            to(other * plane + lax.rem(me + step, half * plane), landing, sent, index, at)
+            return carry
+
+        if index < first:
+            lax.fori_loop(1, n, whole, 0)
+        else:
+            lax.fori_loop(0, half * plane, beyond, 0)
+        for c in range(chunks):
+            if index == min(EARLY_AT + c, first - 1):
+                _, early_sent, early_landing, early_stride, _, early_rows = phases[first + c]
+                at = pl.ds(pl.multiple_of(me * early_stride, early_rows), early_rows)
+                for step in range(1, half * plane):
+                    peer = base * plane + lax.rem(me - base * plane + step, half * plane)
+                    to(peer, early_landing, early_sent, first + c, at)
+
     issued = []
 
     def arrive(index):

time: 173 us -> 173 us (level)
  no operation moved by 1% of the time
where the time goes in v4:
time: 173 us
  Pallas kernels  172 us (99%)
    pallas_call x1, Pallas kernels, shards(): pl.pallas_call(functools.partial(kernel, n, cores, items, parts, chunks),...  170 us

profile of v4, /device:TPU:0, one launch (start us, length us, event | category | flops | bytes accessed | tf_op | source)
XLA Modules:
  0.0 173.0 jit_solution(10635728358458366101)
XLA Ops:
  0.6 169.5 %shard_map.102 = (bf16[128,1024]{1,0:T(8,128)(2,1)S(1)}, bf16[4,2048,256]{2,1,0:T(8,128)(2,1)S(1)}, bf16[8,1024,128]{2,1,0:T(8,128)(2,1)S(1)}) custom-call(bf16[128,1024]{1,0:T(8,128)(2,1)} %tokens_in.1, f32[1,128]{1,0:T(1,128)} %bitcast.8, f32[16,128,512]{2,1,0:T(8,128)} %gate_in.1, f32[16,128,512]{2,1,0:T(8,128)} %up_in.1, f32[16,64,1024]{2,1,0:T(8,128)} %down_in.1, ...), custom_call_target="tpu_custom_call" | custom-call | tf_op jit(solution)/shard_map/pallas_call | solution.py:551
  170.1 2.9 %shard_map.103 = (bf16[128,1024]{1,0:T(8,128)(2,1)}, bf16[2048,512]{1,0:T(8,128)(2,1)}, bf16[2048,512]{1,0:T(8,128)(2,1)}, bf16[1024,1024]{1,0:T(8,128)(2,1)}) custom-call(bf16[128,1024]{1,0:T(8,128)(2,1)S(1)} %get-tuple-element.11.mixed, bf16[4,2048,256]{2,1,0:T(8,128)(2,1)S(1)} %get-tuple-element.12.pair, bf16[8,1024,128]{2,1,0:T(8,128)(2,1)S(1)} %get-tuple-element.13.down), custom_call_target="tpu_custom_call" | custom-call | tf_op jit(solution)/shard_map/pallas_call | solution.py:614
